TPU v7x, 32 devices: a whole 2x2x4 slice. The times are simulated.
32 devices in a mesh: sp: 4 (over y, x), tp: 8 (over z, core).
Axes of the slice: x: 2, y: 2, z: 4, core: 2. Of those that a mesh axis runs over, the one named last changes fastest.
Arguments:
- tokens: bfloat16 [8192, 2048], P('sp', 'tp'), may hold values from -6 to 6
- norm_gain: float32 [2048], replicated, may hold values from 0.1 to 1.9
- w_key: bfloat16 [2048, 1024], P(None, 'tp'), may hold values from -0.125 to 0.125
- w_decay: bfloat16 [2048, 1024], P(None, 'tp'), may hold values from -0.125 to 0.125
- w_value: bfloat16 [2048, 512], replicated, may hold values from -0.125 to 0.125
- decay_bias: float32 [1024], P('tp'), may hold values from 0 to 8.5
- gate_drift: float32 [8192], P('sp'), may hold values from -1 to 1
- queries: bfloat16 [1024], P('tp'), may hold values from -6 to 6
- out_gain: float32 [4, 512], P(None, 'sp'), may hold values from 0.1 to 1.9
Outputs:
- state_cache: bfloat16 [1024, 512], P('tp', 'sp')
- first_read: float32 [4, 512], P(None, 'sp')
All inputs are finite; a program needn't handle non-finite values.
Results may differ from a plain program's by a relative error of at most 0.009.
Values may be sent and summed in bfloat16 or wider, within the bound.
A program may use at most 128 MiB of HBM per device.

v0:
```python
import jax
import jax.numpy as jnp
from jax import lax
from jax.sharding import PartitionSpec as P

QUERY_KEY_HEADS = 4
KEY_CHANNELS = 256
VALUE_CHANNELS = 512
EPS = 1e-06
GATE_NORM = 16.0


def body(tokens, norm_gain, w_key, w_decay, w_value, decay_bias, gate_drift, queries, out_gain):
    gathered = lax.all_gather(tokens, "tp", axis=1, tiled=True)
    rows_f32 = gathered.astype(jnp.float32)
    inverse_rms = lax.rsqrt(jnp.mean(rows_f32 * rows_f32, axis=1, keepdims=True) + EPS)
    normed = (rows_f32 * inverse_rms * norm_gain[None, :]).astype(jnp.bfloat16)
    key_proj = jnp.dot(normed, w_key, preferred_element_type=jnp.float32).astype(jnp.bfloat16)
    gate_pre = jnp.dot(normed, w_decay, preferred_element_type=jnp.float32).astype(jnp.bfloat16)
    value_proj = jnp.dot(normed, w_value, preferred_element_type=jnp.float32).astype(jnp.bfloat16)
    log_decay = (
        jax.nn.log_sigmoid(gate_pre.astype(jnp.float32) + decay_bias[None, :] + gate_drift[:, None])
        / GATE_NORM
    )
    suffix = lax.cumsum(log_decay, axis=0, reverse=True)
    weighted = (key_proj.astype(jnp.float32) * jnp.exp(suffix - log_decay)).astype(jnp.bfloat16)
    partial_value = lax.dot_general(
        weighted, value_proj, (((0,), (0,)), ((), ())), preferred_element_type=jnp.float32
    )
    total_decay = suffix[0]
    channels = partial_value.shape[0]
    span_count = lax.axis_size("sp")
    spread = jnp.broadcast_to(total_decay[None, :, None], (1, channels, span_count))
    blocks, totals = (
        lax.all_to_all(partial_value[None], "sp", split_axis=2, concat_axis=0, tiled=True),
        lax.all_to_all(spread, "sp", split_axis=2, concat_axis=0, tiled=True),
    )
    later_sum = lax.cumsum(totals, axis=0, reverse=True) - totals
    matrix_state = jnp.sum(jnp.exp(later_sum) * blocks, axis=0)
    state_cache = matrix_state.astype(jnp.bfloat16)
    channel_ids = lax.axis_index("tp") * channels + jnp.arange(channels, dtype=jnp.int32)
    owners = (channel_ids // KEY_CHANNELS)[:, None] == jnp.arange(QUERY_KEY_HEADS, dtype=jnp.int32)[
        None, :
    ]
    query_of_head = jnp.where(
        owners, queries.astype(jnp.float32)[:, None] * KEY_CHANNELS ** (-0.5), 0.0
    )
    part_read = lax.dot_general(
        query_of_head, matrix_state, (((0,), (0,)), ((), ())), precision=lax.Precision.HIGHEST
    )
    summed_read = lax.psum(part_read, "tp")
    squares = lax.psum(jnp.sum(summed_read * summed_read, axis=1), "sp")
    first_read = summed_read * lax.rsqrt(squares / VALUE_CHANNELS + EPS)[:, None] * out_gain
    return (state_cache, first_read)


def solution(mesh):
    return jax.shard_map(
        body,
        mesh=mesh,
        in_specs=(
            P("sp", "tp"),
            P(),
            P(None, "tp"),
            P(None, "tp"),
            P(),
            P("tp"),
            P("sp"),
            P("tp"),
            P(None, "sp"),
        ),
        out_specs=(P("tp", "sp"), P(None, "sp")),
        check_vma=False,
    )
```

profile of v0, /device:TPU:0, one launch (start us, length us, event | category | flops | bytes accessed | tf_op | source)
XLA Modules:
  0.0 171.0 jit_solution(2722808447826279931)
XLA Ops:
  7.2 0.0 copy-start
  7.2 0.0 copy-start.5
  7.2 0.0 copy-start.3
  7.2 0.0 copy-start.6
  7.2 0.0 copy-start.4
  7.2 0.0 all-gather.2.cloned.1.call-start
  7.3 0.7 all-gather.2.cloned.1.call-update
  8.0 0.7 convert_multiply_fusion.2
  8.7 86.2 %all-gather.2.cloned.1.call-done = bf16[2048,2048]{1,0:T(8,128)(2,1)} async-done(((bf16[2048,256]{1,0:T(8,128)(2,1)}), bf16[2048,2048]{1,0:T(8,128)(2,1)}) %all-gather.2.cloned.1.call-update) | async-done | bytes 8388624 | tf_op jit(solution)/shard_map/all_gather | solution.py:14
  94.9 5.2 %fusion = f32[2048]{0:T(1024)S(1)} fusion(bf16[2048,2048]{1,0:T(8,128)(2,1)} %all-gather.2.cloned.1.call-done), kind=kLoop, calls=%fused_computation.2 | loop fusion | flops 12580864 | bytes 8396800 | tf_op jit(solution)/shard_map/reduce_sum | solution.py:16
  100.1 0.0 copy-done.5
  100.1 0.0 copy-done.3
  100.1 0.0 copy-done.6
  100.1 0.0 copy-done.4
  100.1 0.5 copy-done.1
  100.6 4.7 %fusion.12 = (f32[128,2048]{0,1:T(8,128)S(1)}, f32[2048,128]{1,0:T(8,128)}) fusion(f32[2048]{0:T(1024)S(1)} %copy-done.4, f32[128]{0:T(128)S(1)} %copy-done.6, bf16[2048,128]{1,0:T(8,128)(2,1)S(1)} %copy-done.3, bf16[2048,2048]{1,0:T(8,128)(2,1)S(1)} %copy-done.1, f32[2048]{0:T(1024)S(1)} %copy-done.5, f32[2048]{0:T(1024)S(1)} %add_rsqrt_fusion), kind=kOutput, calls=%fused_computation.19 | convolution fusion | flops 1093926912 | bytes 11035136 | tf_op jit(solution)/shard_map/dot_general | solution.py:19
  105.4 2.6 %fusion.21 = f32[128,16,128]{0,1,2:T(8,128)S(1)} fusion(f32[128,16,128]{0,2,1:T(8,128)S(1)} %bitcast.44), kind=kOutput, calls=%fused_computation.30 | output fusion | flops 33292288 | bytes 2097152 | tf_op jit(solution)/shard_map/reduce-window
  108.0 0.1 broadcast_add_fusion
  108.1 0.3 copy.17
  108.4 0.6 broadcast_in_dim.19
  109.0 3.6 %all-to-all-start = ((f32[1,128,4]{1,0,2:T(1,128)}), f32[1,128,4]{1,0,2:T(1,128)S(1)}, u32[]{:S(2)}, u32[]{:S(2)}) async-start(f32[1,128,4]{1,0,2:T(1,128)} %broadcast_in_dim.19), calls=%async_computation | async-start | bytes 4096 | tf_op jit(solution)/shard_map/all_to_all | solution.py:36
  112.6 7.6 %fusion.9 = bf16[2048,128]{1,0:T(8,128)(2,1)} fusion(bf16[2048,128]{1,0:T(8,128)(2,1)} %param.11, f32[2048,128]{1,0:T(8,128)S(1)} %bitcast.43, f32[2048,128]{1,0:T(8,128)} %get-tuple-element.5, bf16[2048,2048]{1,0:T(8,128)(2,1)} %all-gather.2.cloned.1.call-done, f32[2048]{0:T(1024)S(1)} %copy-done.5, f32[2048]{0:T(1024)S(1)} %add_rsqrt_fusion), kind=kOutput, calls=%fused_computation.16 | convolution fusion | flops 1093926912 | bytes 11550720 | tf_op jit(solution)/shard_map/dot_general | solution.py:18
  120.2 10.2 %fusion.10 = f32[128,512]{0,1:T(8,128)} fusion(bf16[2048,128]{1,0:T(8,128)(2,1)} %fusion.9, bf16[2048,512]{1,0:T(8,128)(2,1)S(1)} %copy-done, bf16[2048,2048]{1,0:T(8,128)(2,1)} %all-gather.2.cloned.1.call-done, f32[2048]{0:T(1024)S(1)} %copy-done.5, f32[2048]{0:T(1024)S(1)} %add_rsqrt_fusion), kind=kOutput, calls=%fused_computation.17 | convolution fusion | flops 4581228544 | bytes 11288576 | tf_op jit(solution)/shard_map/dot_general | solution.py:27
  130.4 0.0 all-to-all-done
  130.5 4.2 %all-to-all-start.1 = ((f32[1,128,512]{1,0,2:T(1,128)}), f32[1,128,512]{1,0,2:T(1,128)S(1)}, u32[]{:S(2)}, u32[]{:S(2)}) async-start(f32[1,128,512]{1,0,2:T(1,128)} %bitcast.18), calls=%async_computation.1 | async-start | bytes 524288 | tf_op jit(solution)/shard_map/all_to_all | solution.py:35
  134.7 5.3 %all-to-all-done.1 = f32[1,128,512]{1,0,2:T(1,128)S(1)} async-done(((f32[1,128,512]{1,0,2:T(1,128)}), f32[1,128,512]{1,0,2:T(1,128)S(1)}, u32[]{:S(2)}, u32[]{:S(2)}) %all-to-all-start.1) | async-done | bytes 262176 | tf_op jit(solution)/shard_map/all_to_all | solution.py:35
  140.0 0.3 fusion.23
  140.3 13.6 %psum.14 = f32[4,128]{1,0:T(4,128)S(1)} all-reduce(f32[4,128]{1,0:T(4,128)S(1)} %fusion.23), channel_id=1, replica_groups=mesh['sp'=4,'tp'=8] {'tp'}, use_global_device_ids=true, to_apply=%region_5.6 | all-reduce | flops 512 | bytes 4096 | tf_op jit(solution)/shard_map/psum | solution.py:51
  153.9 0.1 multiply_reduce_fusion.1
  154.1 8.7 %psum.15 = f32[4]{0:T(128)S(1)} all-reduce(f32[4]{0:T(128)S(1)} %multiply_reduce_fusion.1), channel_id=1, replica_groups=mesh['sp'=4,'tp'=8] {'sp'}, use_global_device_ids=true, to_apply=%region_7.8 | all-reduce | flops 4 | bytes 32 | tf_op jit(solution)/shard_map/psum | solution.py:52
  162.8 0.7 copy.19
  163.5 0.6 multiply_multiply_fusion
  (15 shorter events, 0.2 us)
Async XLA Ops:
  7.2 113.1 %copy-start = (bf16[2048,512]{1,0:T(8,128)(2,1)S(1)}, bf16[2048,512]{1,0:T(8,128)(2,1)}, u32[]{:S(2)}) copy-start(bf16[2048,512]{1,0:T(8,128)(2,1)} %param.13) | copy-start | bytes 6291460
  7.2 92.9 %copy-start.5 = (f32[2048]{0:T(1024)S(1)}, f32[2048]{0:T(1024)}, u32[]{:S(2)}) copy-start(f32[2048]{0:T(1024)} %param.10) | copy-start | bytes 24580
  7.2 92.9 %copy-start.3 = (bf16[2048,128]{1,0:T(8,128)(2,1)S(1)}, bf16[2048,128]{1,0:T(8,128)(2,1)}, u32[]{:S(2)}) copy-start(bf16[2048,128]{1,0:T(8,128)(2,1)} %param.12) | copy-start | bytes 1572868
  7.2 92.9 %copy-start.6 = (f32[128]{0:T(128)S(1)}, f32[128]{0:T(128)}, u32[]{:S(2)}) copy-start(f32[128]{0:T(128)} %param.14) | copy-start | bytes 1540
  7.2 92.9 %copy-start.4 = (f32[2048]{0:T(1024)S(1)}, f32[2048]{0:T(1024)}, u32[]{:S(2)}) copy-start(f32[2048]{0:T(1024)} %param.15) | copy-start | bytes 24580
  7.2 87.6 %all-gather.2.cloned.1.call-start = ((), (), s32[]{:S(2)}) async-start(), calls=%async_computation.2 | async-start | bytes 9437184 | tf_op jit(solution)/shard_map/all_gather | solution.py:14
  94.9 5.8 %copy-start.1 = (bf16[2048,2048]{1,0:T(8,128)(2,1)S(1)}, bf16[2048,2048]{1,0:T(8,128)(2,1)}, u32[]{:S(2)}) copy-start(bf16[2048,2048]{1,0:T(8,128)(2,1)} %all-gather.2.cloned.1.call-done) | copy-start | bytes 25165828
  109.0 21.5 %all-to-all-start = ((f32[1,128,4]{1,0,2:T(1,128)}), f32[1,128,4]{1,0,2:T(1,128)S(1)}, u32[]{:S(2)}, u32[]{:S(2)}) async-start(f32[1,128,4]{1,0,2:T(1,128)} %broadcast_in_dim.19), calls=%async_computation | async-start | bytes 4096 | tf_op jit(solution)/shard_map/all_to_all | solution.py:36
  120.2 43.3 %copy-start.2 = (f32[4,128]{1,0:T(4,128)S(1)}, f32[4,128]{1,0:T(4,128)}, u32[]{:S(2)}) copy-start(f32[4,128]{1,0:T(4,128)} %param.17) | copy-start | bytes 6148
  130.5 9.6 %all-to-all-start.1 = ((f32[1,128,512]{1,0,2:T(1,128)}), f32[1,128,512]{1,0,2:T(1,128)S(1)}, u32[]{:S(2)}, u32[]{:S(2)}) async-start(f32[1,128,512]{1,0,2:T(1,128)} %bitcast.18), calls=%async_computation.1 | async-start | bytes 524288 | tf_op jit(solution)/shard_map/all_to_all | solution.py:35
Sparse Core Ops, SparseCore 0:
  9.6 85.1 all-gather.1
where the time goes:
time: 171 us
  waiting for transfers between devices  92.2 us (54%)
  matrix products  22.8 us (13%)
  blocking collectives  22.4 us (13%)
  between operations  14.2 us (8%)
  other arithmetic  9.45 us (6%)
  starting transfers between devices  7.88 us (5%)
  local copies, waits for them, and re-layouts  2.17 us (1%)
    all_gather x1, waiting for transfers between devices, body(): gathered = lax.all_gather(tokens, 'tp', axis=1, tiled=True)  86.2 us
    psum x1, blocking collectives, body(): summed_read = lax.psum(part_read, 'tp')  13.6 us
    dot_general x1, matrix products, body(): lax.dot_general(weighted, value_proj, (((0,), (0,)), ((), ())), preferred...  10.2 us
    psum x1, blocking collectives, body(): squares = lax.psum(jnp.sum(summed_read * summed_read, axis=1), 'sp')  8.74 us
    dot_general x1, matrix products, body(): jnp.dot(normed, w_key, preferred_element_type=jnp.float32)  7.58 us
    all_to_all x1, waiting for transfers between devices, body(): lax.all_to_all(partial_value[None], 'sp', split_axis=2, concat_axis=0, ti...  5.33 us
    reduce_sum x1, other arithmetic, body(): jnp.mean(rows_f32 * rows_f32, axis=1, keepdims=True) + EPS  5.23 us
    dot_general x1, matrix products, body(): jnp.dot(normed, w_decay, preferred_element_type=jnp.float32)  4.74 us
  transfers between devices with their start and end apart: 3, of which 2 were waited for; matrix products, arithmetic and copies ran while one was open for 11% of the time, Pallas kernels for 0%

commit v1 on v0

--- a/solution.py
+++ b/solution.py
@@ -48,7 +48,11 @@
     part_read = lax.dot_general(
         query_of_head, matrix_state, (((0,), (0,)), ((), ())), precision=lax.Precision.HIGHEST
     )
-    summed_read = lax.psum(part_read, "tp")
+    summed_read = part_read
+    for hop in (1, 2, 4):
+        summed_read = summed_read + lax.ppermute(
+            summed_read, "tp", [(dev, dev ^ hop) for dev in range(8)]
+        )
     squares = lax.psum(jnp.sum(summed_read * summed_read, axis=1), "sp")
     first_read = summed_read * lax.rsqrt(squares / VALUE_CHANNELS + EPS)[:, None] * out_gain
     return (state_cache, first_read)

time: 171 us -> 166 us (0.971)
  blocking collectives: 22.4 us -> 8.73 us
  waiting for transfers between devices: 92.2 us -> 98.9 us
  starting transfers between devices: 7.88 us -> 9.7 us
    psum x1 -> x0, blocking collectives: 13.6 us -> none  [body(): summed_read = lax.psum(part_read, 'tp')]
    ppermute x0 -> x3, waiting for transfers between devices: none -> 6.72 us  [body(): lax.ppermute(summed_read, 'tp', [(dev, dev ^ hop) for dev in range(8)])]
    ppermute x0 -> x3, starting transfers between devices: none -> 1.82 us  [body(): lax.ppermute(summed_read, 'tp', [(dev, dev ^ hop) for dev in range(8)])]
  transfers between devices with their start and end apart: 3 -> 6, of which waited for: 2 -> 5; matrix products, arithmetic and copies ran while one was open for 11% -> 12% of each run, Pallas kernels for 0% -> 0%
where the time goes in v1:
time: 166 us
  waiting for transfers between devices  98.9 us (60%)
  matrix products  22.8 us (14%)
  between operations  14.2 us (9%)
  starting transfers between devices  9.7 us (6%)
  other arithmetic  9.46 us (6%)
  blocking collectives  8.73 us (5%)
  local copies, waits for them, and re-layouts  2.17 us (1%)
    all_gather x1, waiting for transfers between devices, body(): gathered = lax.all_gather(tokens, 'tp', axis=1, tiled=True)  86.2 us
    dot_general x1, matrix products, body(): lax.dot_general(weighted, value_proj, (((0,), (0,)), ((), ())), preferred...  10.2 us
    psum x1, blocking collectives, body(): squares = lax.psum(jnp.sum(summed_read * summed_read, axis=1), 'sp')  8.73 us
    dot_general x1, matrix products, body(): jnp.dot(normed, w_key, preferred_element_type=jnp.float32)  7.58 us
    ppermute x3, waiting for transfers between devices, body(): lax.ppermute(summed_read, 'tp', [(dev, dev ^ hop) for dev in range(8)])  6.72 us
    all_to_all x1, waiting for transfers between devices, body(): lax.all_to_all(partial_value[None], 'sp', split_axis=2, concat_axis=0, ti...  5.33 us
    reduce_sum x1, other arithmetic, body(): jnp.mean(rows_f32 * rows_f32, axis=1, keepdims=True) + EPS  5.23 us
    dot_general x1, matrix products, body(): jnp.dot(normed, w_decay, preferred_element_type=jnp.float32)  4.74 us
  transfers between devices with their start and end apart: 6, of which 5 were waited for; matrix products, arithmetic and copies ran while one was open for 12% of the time, Pallas kernels for 0%

profile of v1, /device:TPU:0, one launch (start us, length us, event | category | flops | bytes accessed | tf_op | source)
XLA Modules:
  0.0 166.0 jit_solution(4445848222266797332)
XLA Ops:
  7.2 0.0 copy-start
  7.2 0.0 copy-start.5
  7.2 0.0 copy-start.3
  7.2 0.0 copy-start.6
  7.2 0.0 all-gather.2.cloned.1.call-start
  7.3 0.7 all-gather.2.cloned.1.call-update
  8.0 0.7 convert_multiply_fusion.2
  8.7 86.2 %all-gather.2.cloned.1.call-done = bf16[2048,2048]{1,0:T(8,128)(2,1)} async-done(((bf16[2048,256]{1,0:T(8,128)(2,1)}), bf16[2048,2048]{1,0:T(8,128)(2,1)}) %all-gather.2.cloned.1.call-update) | async-done | bytes 8388624 | tf_op jit(solution)/shard_map/all_gather | solution.py:14
  94.9 5.2 %fusion = f32[2048]{0:T(1024)S(1)} fusion(bf16[2048,2048]{1,0:T(8,128)(2,1)} %all-gather.2.cloned.1.call-done), kind=kLoop, calls=%fused_computation.2 | loop fusion | flops 12580864 | bytes 8396800 | tf_op jit(solution)/shard_map/reduce_sum | solution.py:16
  100.1 0.5 copy-done.1
  100.6 4.7 %fusion.12 = (f32[128,2048]{0,1:T(8,128)S(1)}, f32[2048,128]{1,0:T(8,128)}) fusion(f32[2048]{0:T(1024)S(1)} %copy-done.4, f32[128]{0:T(128)S(1)} %copy-done.6, bf16[2048,128]{1,0:T(8,128)(2,1)S(1)} %copy-done.3, bf16[2048,2048]{1,0:T(8,128)(2,1)S(1)} %copy-done.1, f32[2048]{0:T(1024)S(1)} %copy-done.5, f32[2048]{0:T(1024)S(1)} %add_rsqrt_fusion), kind=kOutput, calls=%fused_computation.19 | convolution fusion | flops 1093926912 | bytes 11035136 | tf_op jit(solution)/shard_map/dot_general | solution.py:19
  105.4 2.6 %fusion.21 = f32[128,16,128]{0,1,2:T(8,128)S(1)} fusion(f32[128,16,128]{0,2,1:T(8,128)S(1)} %bitcast.44), kind=kOutput, calls=%fused_computation.30 | output fusion | flops 33292288 | bytes 2097152 | tf_op jit(solution)/shard_map/reduce-window
  108.0 0.1 broadcast_add_fusion
  108.1 0.3 copy.17
  108.4 0.6 broadcast_in_dim.19
  109.0 3.6 %all-to-all-start = ((f32[1,128,4]{1,0,2:T(1,128)}), f32[1,128,4]{1,0,2:T(1,128)S(1)}, u32[]{:S(2)}, u32[]{:S(2)}) async-start(f32[1,128,4]{1,0,2:T(1,128)} %broadcast_in_dim.19), calls=%async_computation | async-start | bytes 4096 | tf_op jit(solution)/shard_map/all_to_all | solution.py:36
  112.6 7.6 %fusion.9 = bf16[2048,128]{1,0:T(8,128)(2,1)} fusion(bf16[2048,128]{1,0:T(8,128)(2,1)} %param.11, f32[2048,128]{1,0:T(8,128)S(1)} %bitcast.43, f32[2048,128]{1,0:T(8,128)} %get-tuple-element.7, bf16[2048,2048]{1,0:T(8,128)(2,1)} %all-gather.2.cloned.1.call-done, f32[2048]{0:T(1024)S(1)} %copy-done.5, f32[2048]{0:T(1024)S(1)} %add_rsqrt_fusion), kind=kOutput, calls=%fused_computation.16 | convolution fusion | flops 1093926912 | bytes 11550720 | tf_op jit(solution)/shard_map/dot_general | solution.py:18
  120.2 10.2 %fusion.10 = f32[128,512]{0,1:T(8,128)} fusion(bf16[2048,128]{1,0:T(8,128)(2,1)} %fusion.9, bf16[2048,512]{1,0:T(8,128)(2,1)S(1)} %copy-done, bf16[2048,2048]{1,0:T(8,128)(2,1)} %all-gather.2.cloned.1.call-done, f32[2048]{0:T(1024)S(1)} %copy-done.5, f32[2048]{0:T(1024)S(1)} %add_rsqrt_fusion), kind=kOutput, calls=%fused_computation.17 | convolution fusion | flops 4581228544 | bytes 11288576 | tf_op jit(solution)/shard_map/dot_general | solution.py:27
  130.4 0.0 all-to-all-done
  130.5 4.2 %all-to-all-start.1 = ((f32[1,128,512]{1,0,2:T(1,128)}), f32[1,128,512]{1,0,2:T(1,128)S(1)}, u32[]{:S(2)}, u32[]{:S(2)}) async-start(f32[1,128,512]{1,0,2:T(1,128)} %bitcast.18), calls=%async_computation.1 | async-start | bytes 524288 | tf_op jit(solution)/shard_map/all_to_all | solution.py:35
  134.7 5.3 %all-to-all-done.1 = f32[1,128,512]{1,0,2:T(1,128)S(1)} async-done(((f32[1,128,512]{1,0,2:T(1,128)}), f32[1,128,512]{1,0,2:T(1,128)S(1)}, u32[]{:S(2)}, u32[]{:S(2)}) %all-to-all-start.1) | async-done | bytes 262176 | tf_op jit(solution)/shard_map/all_to_all | solution.py:35
  140.0 0.3 fusion.23
  140.3 0.0 collective-permute-start
  140.3 1.2 collective-permute-done
  141.5 0.0 collective-permute-start.1
  141.5 3.6 %collective-permute-done.1 = f32[4,128]{1,0:T(4,128)S(1)} collective-permute-done((f32[4,128]{1,0:T(4,128)S(1)}, f32[4,128]{1,0:T(4,128)S(1)}, u32[]{:S(2)}, u32[]{:S(2)}) %collective-permute-start.1) | collective-permute-done | bytes 2080 | tf_op jit(solution)/shard_map/ppermute | solution.py:53
  145.1 1.8 %collective-permute-start.2 = (f32[4,128]{1,0:T(4,128)S(1)}, f32[4,128]{1,0:T(4,128)S(1)}, u32[]{:S(2)}, u32[]{:S(2)}) collective-permute-start(f32[4,128]{1,0:T(4,128)S(1)} %add.82), channel_id=1, source_target_pairs={{0,4},{1,5},{2,6},{3,7},{4,0},{5,1},{6,2},{7,3},{8,12},{9,13},{10,... | collective-permute-start | bytes 6152 | tf_op jit(solution)/shard_map/ppermute | solution.py:53
  146.9 0.7 copy.19
  147.7 1.9 %collective-permute-done.2 = f32[4,128]{1,0:T(4,128)S(1)} collective-permute-done((f32[4,128]{1,0:T(4,128)S(1)}, f32[4,128]{1,0:T(4,128)S(1)}, u32[]{:S(2)}, u32[]{:S(2)}) %collective-permute-start.2) | collective-permute-done | bytes 2080 | tf_op jit(solution)/shard_map/ppermute | solution.py:53
  149.6 0.1 multiply_reduce_fusion.1
  149.7 8.7 %psum.7 = f32[4]{0:T(128)S(1)} all-reduce(f32[4]{0:T(128)S(1)} %get-tuple-element.4), channel_id=1, replica_groups=mesh['sp'=4,'tp'=8] {'sp'}, use_global_device_ids=true, to_apply=%region_6.7 | all-reduce | flops 4 | bytes 32 | tf_op jit(solution)/shard_map/psum | solution.py:56
  158.5 0.7 multiply_multiply_fusion
  (22 shorter events, 0.2 us)
Async XLA Ops:
  7.2 113.1 %copy-start = (bf16[2048,512]{1,0:T(8,128)(2,1)S(1)}, bf16[2048,512]{1,0:T(8,128)(2,1)}, u32[]{:S(2)}) copy-start(bf16[2048,512]{1,0:T(8,128)(2,1)} %param.13) | copy-start | bytes 6291460
  7.2 92.9 %copy-start.5 = (f32[2048]{0:T(1024)S(1)}, f32[2048]{0:T(1024)}, u32[]{:S(2)}) copy-start(f32[2048]{0:T(1024)} %param.10) | copy-start | bytes 24580
  7.2 92.9 %copy-start.3 = (bf16[2048,128]{1,0:T(8,128)(2,1)S(1)}, bf16[2048,128]{1,0:T(8,128)(2,1)}, u32[]{:S(2)}) copy-start(bf16[2048,128]{1,0:T(8,128)(2,1)} %param.12) | copy-start | bytes 1572868
  7.2 92.9 %copy-start.6 = (f32[128]{0:T(128)S(1)}, f32[128]{0:T(128)}, u32[]{:S(2)}) copy-start(f32[128]{0:T(128)} %param.14) | copy-start | bytes 1540
  7.2 92.9 %copy-start.4 = (f32[2048]{0:T(1024)S(1)}, f32[2048]{0:T(1024)}, u32[]{:S(2)}) copy-start(f32[2048]{0:T(1024)} %param.15) | copy-start | bytes 24580
  7.2 87.6 %all-gather.2.cloned.1.call-start = ((), (), s32[]{:S(2)}) async-start(), calls=%async_computation.2 | async-start | bytes 9437184 | tf_op jit(solution)/shard_map/all_gather | solution.py:14
  94.9 5.8 %copy-start.1 = (bf16[2048,2048]{1,0:T(8,128)(2,1)S(1)}, bf16[2048,2048]{1,0:T(8,128)(2,1)}, u32[]{:S(2)}) copy-start(bf16[2048,2048]{1,0:T(8,128)(2,1)} %all-gather.2.cloned.1.call-done) | copy-start | bytes 25165828
  109.0 21.5 %all-to-all-start = ((f32[1,128,4]{1,0,2:T(1,128)}), f32[1,128,4]{1,0,2:T(1,128)S(1)}, u32[]{:S(2)}, u32[]{:S(2)}) async-start(f32[1,128,4]{1,0,2:T(1,128)} %broadcast_in_dim.19), calls=%async_computation | async-start | bytes 4096 | tf_op jit(solution)/shard_map/all_to_all | solution.py:36
  120.2 38.2 %copy-start.2 = (f32[4,128]{1,0:T(4,128)S(1)}, f32[4,128]{1,0:T(4,128)}, u32[]{:S(2)}) copy-start(f32[4,128]{1,0:T(4,128)} %param.17) | copy-start | bytes 6148
  130.5 9.6 %all-to-all-start.1 = ((f32[1,128,512]{1,0,2:T(1,128)}), f32[1,128,512]{1,0,2:T(1,128)S(1)}, u32[]{:S(2)}, u32[]{:S(2)}) async-start(f32[1,128,512]{1,0,2:T(1,128)} %bitcast.18), calls=%async_computation.1 | async-start | bytes 524288 | tf_op jit(solution)/shard_map/all_to_all | solution.py:35
  140.3 1.2 collective-permute-start
  141.5 3.6 %collective-permute-start.1 = (f32[4,128]{1,0:T(4,128)S(1)}, f32[4,128]{1,0:T(4,128)S(1)}, u32[]{:S(2)}, u32[]{:S(2)}) collective-permute-start(f32[4,128]{1,0:T(4,128)S(1)} %add.81), channel_id=1, source_target_pairs={{0,2},{1,3},{2,0},{3,1},{4,6},{5,7},{6,4},{7,5},{8,10},{9,11},{10,... | collective-permute-start | bytes 6152 | tf_op jit(solution)/shard_map/ppermute | solution.py:53
  145.1 4.5 %collective-permute-start.2 = (f32[4,128]{1,0:T(4,128)S(1)}, f32[4,128]{1,0:T(4,128)S(1)}, u32[]{:S(2)}, u32[]{:S(2)}) collective-permute-start(f32[4,128]{1,0:T(4,128)S(1)} %add.82), channel_id=1, source_target_pairs={{0,4},{1,5},{2,6},{3,7},{4,0},{5,1},{6,2},{7,3},{8,12},{9,13},{10,... | collective-permute-start | bytes 6152 | tf_op jit(solution)/shard_map/ppermute | solution.py:53
Sparse Core Ops, SparseCore 0:
  9.6 85.1 all-gather.1
